TPU v7x, 32 devices: a whole 2x2x4 slice. The times are simulated.
32 devices in a mesh: sp: 4 (over z), dp: 8 (over y, x, core).
Axes of the slice: x: 2, y: 2, z: 4, core: 2. Of those that a mesh axis runs over, the one named last changes fastest.
Arguments:
- queries: bfloat16 [8, 768, 1024], P('dp', 'sp'), may hold values from -6 to 6
- keys: bfloat16 [8, 768, 256], P('dp', 'sp'), may hold values from -6 to 6
- values: bfloat16 [8, 768, 256], P('dp', 'sp'), may hold values from -6 to 6
- query_gain: float32 [64], replicated, may hold values from 0.15 to 7
- key_gain: float32 [64], replicated, may hold values from 0.15 to 7
- out_weight: bfloat16 [1024, 2048], P(None, 'dp'), may hold values from -0.1875 to 0.1875
- out_gain: float32 [2048], replicated, may hold values from 0.1 to 1.9
Outputs:
- output: bfloat16 [8, 768, 2048], P('dp', 'sp')
All inputs are finite; a program needn't handle non-finite values.
Results may differ from a plain program's by a relative error of at most 0.0035.
The roundings to bfloat16 on the way count: a program that leaves them out, or rounds other values in their place, can miss the bound.
Values may be sent and summed in bfloat16 or wider, within the bound.
A program may use at most 64 MiB of HBM per device.

v0:
```python
import functools

import jax
import jax.numpy as jnp
import numpy as np
from jax import lax
from jax.experimental import pallas as pl
from jax.experimental.pallas import tpu as pltpu
from jax.sharding import PartitionSpec as P

QH = 16
KVH = 4
HEAD = 64
GRID_W = 64
GROUP = QH // KVH
HALVES = 2
BLOCK = GROUP * HEAD


EPSILON = 1e-06
ROTARY_BASE = 10000.0

F32 = jnp.float32
BF16 = jnp.bfloat16


def rotate(vectors, positions, width):
    half_width = width // 2
    frequency = ROTARY_BASE ** (-jnp.arange(0, width, 2, dtype=jnp.float32) / width)
    angles = positions.astype(jnp.float32)[:, None] * frequency[None, :]
    cosines = jnp.cos(angles)[:, None, :]
    sine_table = jnp.sin(angles)[:, None, :]
    first_half = vectors[..., :half_width]
    second_half = vectors[..., half_width:]
    return jnp.concatenate(
        [
            first_half * cosines - second_half * sine_table,
            second_half * cosines + first_half * sine_table,
        ],
        axis=-1,
    )


def prepare(vectors, gain_vector, grid_row, grid_col):
    vectors = vectors.astype(jnp.float32)
    vectors = (
        vectors
        * lax.rsqrt(jnp.mean(vectors * vectors, axis=-1, keepdims=True) + EPSILON)
        * gain_vector
    )
    half_width = HEAD // 2
    turned = jnp.concatenate(
        [
            rotate(vectors[..., :half_width], grid_row, half_width),
            rotate(vectors[..., half_width:], grid_col, half_width),
        ],
        axis=-1,
    )
    return turned.astype(jnp.bfloat16)


def softmax_rows(scores):
    row_max = jnp.max(scores, axis=-1, keepdims=True)
    exponent = jnp.exp(scores - row_max)
    return exponent / jnp.sum(exponent, axis=-1, keepdims=True)


def per_device_general(queries, keys, values, query_gain, key_gain, out_weight, out_gain):
    sp_count = lax.axis_size("sp")
    tokens_here = queries.shape[1]
    seq_len = tokens_here * sp_count
    score_scale = HEAD ** (-0.5)
    offset = lax.axis_index("sp") * tokens_here
    positions = offset + jnp.arange(tokens_here, dtype=jnp.int32)
    grid_row = positions // GRID_W
    grid_col = positions % GRID_W
    query_rot = prepare(queries[0].reshape(tokens_here, QH, HEAD), query_gain, grid_row, grid_col)
    key_rot = prepare(keys[0].reshape(tokens_here, KVH, HEAD), key_gain, grid_row, grid_col)
    value_heads = values[0].reshape(tokens_here, KVH, HEAD)
    kv_pairs = jnp.concatenate([key_rot, value_heads], axis=2)
    all_pairs = lax.all_gather(
        kv_pairs.reshape(tokens_here, KVH * 2 * HEAD), "sp", axis=0, tiled=True
    )
    all_pairs = all_pairs.reshape(seq_len, KVH, 2, HEAD)
    key_all = all_pairs[:, :, 0].transpose(1, 0, 2)
    value_all = all_pairs[:, :, 1].transpose(1, 0, 2)
    query_groups = query_rot.reshape(tokens_here, KVH, QH // KVH, HEAD).transpose(1, 0, 2, 3)

    def attend_group(operands):
        query_group, key_head, value_head = operands
        scores = (
            jnp.einsum("qgd,kd->gqk", query_group, key_head, preferred_element_type=jnp.float32)
            * score_scale
        )
        attn_weights = softmax_rows(scores).astype(jnp.bfloat16)
        return jnp.einsum(
            "gqk,kd->qgd", attn_weights, value_head, preferred_element_type=jnp.float32
        ).astype(jnp.bfloat16)

    results = lax.map(attend_group, (query_groups, key_all, value_all))
    attended = results.transpose(1, 0, 2, 3).reshape(tokens_here, QH * HEAD)
    projected = jnp.dot(
        attended,
        lax.all_gather(out_weight, "dp", axis=1, tiled=True),
        preferred_element_type=jnp.float32,
    )
    normed = (
        projected
        * lax.rsqrt(jnp.mean(projected * projected, axis=-1, keepdims=True) + EPSILON)
        * out_gain
    )
    return normed.astype(jnp.bfloat16)[None]


def position_tables(seq_len):
    width = HEAD // 2
    frequency = np.float32(ROTARY_BASE) ** (
        -np.arange(0, width, 2, dtype=np.float32) / np.float32(width)
    )
    position = np.arange(seq_len)
    parts = []
    for coordinate in (position // GRID_W, position % GRID_W):
        angles = coordinate.astype(np.float32)[:, None] * frequency[None, :]
        parts += [angles, angles]
    angles = np.concatenate(parts * 2, axis=1).astype(np.float64)
    return np.stack([np.cos(angles), np.sin(angles)]).astype(np.float32)


def dot(a, b):
    return jnp.dot(a, b, preferred_element_type=F32)


def cross(a, b):
    return lax.dot_general(a, b, (((1,), (1,)), ((), ())), preferred_element_type=F32)


def kernel(
    sp, dp,
    q_ref, k_ref, v_ref, qg_ref, kg_ref, w_ref, og_ref, table_ref,
    out_ref,
    q_raw, q_rot, k_all, v_all, tables, w_all, gains,
    swap_mat, ones_mat, place_mat, back_mat, v_turned,
    expo, peak, total, att, proj,
    local_sem, kv_send, kv_recv, w_send, w_recv,
):
    tokens = q_raw.shape[0]
    depth = w_ref.shape[0]
    half = depth // 2
    me = lax.axis_index("sp")
    here = lax.axis_index("dp")
    mate = here + 1 - 2 * (here % 2)
    flip_x = 2 - 4 * ((here // 2) % 2)
    flip_y = 4 - 8 * ((here // 4) % 2)
    dev_x = here + flip_x
    dev_y = here + flip_y
    dev_d = here + flip_x + flip_y

    barrier = pltpu.get_barrier_semaphore()
    has_left = me > 0
    has_right = me < sp - 1

    for other in (mate, dev_x, dev_y):
        pl.semaphore_signal(barrier, inc=1, device_id={"dp": other})

    @pl.when(has_left)
    def _():
        pl.semaphore_signal(barrier, inc=1, device_id={"sp": me - 1})

    @pl.when(has_right)
    def _():
        pl.semaphore_signal(barrier, inc=1, device_id={"sp": me + 1})

    locals_ = [
        pltpu.make_async_copy(q_ref, q_raw, local_sem.at[0]),
        pltpu.make_async_copy(table_ref, tables, local_sem.at[1]),
        pltpu.make_async_copy(k_ref, k_all.at[pl.ds(me * tokens, tokens)], local_sem.at[2]),
        pltpu.make_async_copy(v_ref, v_all.at[pl.ds(me * tokens, tokens)], local_sem.at[3]),
        pltpu.make_async_copy(w_ref, w_all.at[here], local_sem.at[4]),
    ]
    for copy in locals_:
        copy.start()

    pl.semaphore_wait(barrier, 3 + jnp.minimum(me, 1) + jnp.minimum(sp - 1 - me, 1))

    part = k_ref.shape[1] // HALVES

    def kv_copies(way, step, side):
        block = me - step if way == 0 else me + step
        target = me + 1 if way == 0 else me - 1
        rows = pl.ds(block * tokens, tokens)
        columns = pl.ds(side * part, part)
        copies = []
        for i, (own, every) in enumerate(((k_ref, k_all), (v_ref, v_all))):
            copies.append(
                pltpu.make_async_remote_copy(
                    src_ref=own.at[:, columns] if step == 0 else every.at[rows, columns],
                    dst_ref=every.at[rows, columns],
                    send_sem=kv_send.at[way, step, side, i],
                    recv_sem=kv_recv.at[way, step, side, i],
                    device_id={"sp": target},
                )
            )
        return copies

    def kv_sends(way, step):
        if way == 0:
            return jnp.logical_and(has_right, me - step >= 0)
        return jnp.logical_and(has_left, me + step < sp)

    def kv_start(step, side):
        if step >= sp - 1:
            return
        for way in (0, 1):
            @pl.when(kv_sends(way, step))
            def _(way=way):
                for copy in kv_copies(way, step, side):
                    copy.start()

    def kv_arrive(step, side):
        for way in (0, 1):
            source = me - 1 - step if way == 0 else me + 1 + step
            arrives = source >= 0 if way == 0 else source < sp

            @pl.when(arrives)
            def _(way=way, source=source):
                window = (pl.ds(source * tokens, tokens), pl.ds(side * part, part))
                for i, every in enumerate((k_all, v_all)):
                    pltpu.make_async_remote_copy(
                        src_ref=every.at[window],
                        dst_ref=every.at[window],
                        send_sem=kv_send.at[way, step, side, i],
                        recv_sem=kv_recv.at[way, step, side, i],
                        device_id={"sp": me},
                    ).wait_recv()
        kv_start(step + 1, side)

    for side in range(HALVES):
        kv_start(0, side)

    top, bottom, whole = (0, half), (half, half), (0, depth)

    def w_copy(index, shard, rows, target, own=False):
        window = pl.ds(rows[0], rows[1])
        return pltpu.make_async_remote_copy(
            src_ref=w_ref.at[window] if own else w_all.at[shard, window],
            dst_ref=w_all.at[shard, window],
            send_sem=w_send.at[index],
            recv_sem=w_recv.at[index],
            device_id={"dp": target},
        )

    def w_wait(index, shard, rows):
        w_copy(index, shard, rows, mate).wait_recv()

    sent = [
        w_copy(0, here, bottom, dev_x, own=True),
        w_copy(2, here, top, dev_y, own=True),
        w_copy(1, here, top, dev_x, own=True),
        w_copy(3, here, bottom, dev_y, own=True),
        w_copy(6, here, whole, mate, own=True),
    ]
    for copy in sent:
        copy.start()

    def w_forward(index, shard, rows, target):
        copy = w_copy(index, shard, rows, target)
        copy.start()
        sent.append(copy)

    row_id = lax.broadcasted_iota(jnp.int32, (BLOCK, BLOCK), 0)
    col_id = lax.broadcasted_iota(jnp.int32, (BLOCK, BLOCK), 1)
    quarter = HEAD // 4
    second = (col_id & (HEAD // 2 - 1)) >= quarter
    partner_col = jnp.where(second, col_id - quarter, col_id + quarter)
    hit = row_id == partner_col
    swap_mat[...] = jnp.where(hit, jnp.where(second, 1.0, -1.0), 0.0).astype(BF16)
    ones_mat[...] = jnp.where((row_id // HEAD) == (col_id // HEAD), 1.0, 0.0).astype(BF16)
    spread = jnp.where(
        row_id[:HEAD] == (col_id[:HEAD] & (HEAD - 1)), 1.0, 0.0
    ).astype(BF16)
    spread_swapped = jnp.where(
        row_id[:HEAD] == (partner_col[:HEAD] & (HEAD - 1)), 1.0, 0.0
    ).astype(BF16)
    for i, gain_ref in enumerate((qg_ref, kg_ref)):
        gain = jnp.broadcast_to(gain_ref[...], (16, HEAD))
        first = gain.astype(BF16)
        rest = gain - first.astype(F32)
        mid = rest.astype(BF16)
        low = (rest - mid.astype(F32)).astype(BF16)
        for j, matrix in enumerate((spread, spread_swapped)):
            gains[2 * i + j] = (dot(first, matrix) + dot(mid, matrix)) + dot(low, matrix)

    lane_head = lax.broadcasted_iota(jnp.int32, (1, BLOCK), 1) // HEAD
    masks = [jnp.where(lane_head == p, 1.0, 0.0) for p in range(GROUP)]

    def turned(x, rows, which, scale):
        xf = x.astype(F32)
        square = xf * xf
        high = square.astype(BF16)
        low = (square - high.astype(F32)).astype(BF16)
        size = x.shape[1]
        ones = ones_mat[:size, :size]
        mean = (dot(high, ones) + dot(low, ones)) * (1.0 / HEAD)
        inverse = lax.rsqrt(mean + EPSILON) * scale
        swapped = dot(x, swap_mat[:size, :size])
        cosines = tables[0, rows, :]
        sines = tables[1, rows, :]
        if size > 2 * HEAD:
            cosines = jnp.concatenate([cosines, cosines], axis=1)
            sines = jnp.concatenate([sines, sines], axis=1)
        cosines = cosines * gains[2 * which, 0:1, :size]
        sines = sines * gains[2 * which + 1, 0:1, :size]
        return ((xf * cosines + swapped * sines) * inverse).astype(BF16)

    locals_[0].wait()
    locals_[1].wait()
    own_rows = pl.ds(pl.multiple_of(me * tokens, 64), tokens)
    for b in range(KVH):
        columns = slice(b * BLOCK, (b + 1) * BLOCK)
        q_rot[:, columns] = turned(q_raw[:, columns], own_rows, 0, HEAD ** (-0.5))

    pairs = sp // 2
    mine = me // 2

    eye = jnp.where(row_id == col_id, 1.0, 0.0).astype(BF16)
    wide = GROUP * tokens
    lane = lax.broadcasted_iota(jnp.int32, (BLOCK, wide), 1)
    line = lax.broadcasted_iota(jnp.int32, (BLOCK, wide), 0) // HEAD * tokens
    inside = jnp.logical_and(lane >= line, lane < line + tokens)
    place_mat[...] = jnp.where(inside, 1.0, 0.0).astype(BF16)
    lane = lax.broadcasted_iota(jnp.int32, (tokens, wide), 1)
    line = lax.broadcasted_iota(jnp.int32, (tokens, wide), 0)
    hit = lane == line
    for p in range(1, GROUP):
        hit = jnp.logical_or(hit, lane == line + p * tokens)
    back_mat[...] = jnp.where(hit, 1.0, 0.0).astype(BF16)

    def attend(turn, side):
        span = 2 * tokens
        pair = lax.rem(mine + turn, pairs)
        rows = pl.ds(pl.multiple_of(pair * span, 128), span)
        lanes = slice(side * part, (side + 1) * part)
        key_side = turned(k_all[rows, lanes], rows, 1, 1.0)
        v_turned[turn, lanes, :] = cross(eye[:part, :part], v_all[rows, lanes]).astype(BF16)
        heads = KVH // HALVES

        def one(b):
            columns = slice(b * BLOCK, (b + 1) * BLOCK)
            value_rows = slice(b * HEAD, (b + 1) * HEAD)
            source = (b - side * heads) * HEAD + (col_id[:part] & (HEAD - 1))
            pick = jnp.where(row_id[:part] == source, 1.0, 0.0).astype(BF16)
            key = dot(key_side, pick).astype(BF16)
            query = q_rot[:, columns]
            query = jnp.concatenate([query * mask.astype(BF16) for mask in masks], axis=0)
            scores = cross(key, query)
            high = jnp.max(scores, axis=0, keepdims=True)
            if turn < pairs - 1:
                weights = jnp.exp(scores - high)
                expo[turn, b] = weights
                peak[turn, b] = high
                total[turn, b] = jnp.sum(weights, axis=0, keepdims=True)
                return
            for t in range(turn):
                high = jnp.maximum(high, peak[t, b])
            weights = jnp.exp(scores - high)
            norm = jnp.sum(weights, axis=0, keepdims=True)
            keeps = [jnp.exp(peak[t, b] - high) for t in range(turn)]
            for t in range(turn):
                norm = norm + total[t, b] * keeps[t]
            inverse = 1.0 / norm
            product = dot(v_turned[turn, value_rows, :], (weights * inverse).astype(BF16))
            for t in range(turn):
                old = expo[t, b] * (keeps[t] * inverse)
                product = product + dot(v_turned[t, value_rows, :], old.astype(BF16))
            product = product.astype(BF16)
            placed = jnp.concatenate([product] * GROUP, axis=0) * place_mat[...]
            att[:, columns] = cross(back_mat[...], placed).astype(BF16)

        for b in range(side * heads, (side + 1) * heads):
            one(b)

    locals_[2].wait()
    locals_[3].wait()

    last = HALVES - 1
    for side in range(HALVES):
        kv_arrive(0, side)
    for side in range(last):
        attend(0, side)

    w_wait(0, dev_x, bottom)
    w_forward(5, dev_x, bottom, dev_y)
    w_wait(2, dev_y, top)
    w_forward(4, dev_y, top, dev_x)
    w_forward(7, dev_x, bottom, mate)
    w_forward(9, dev_y, top, mate)
    for step in range(1, sp - 2):
        for side in range(HALVES):
            kv_arrive(step, side)

    attend(0, last)
    if sp > 2:
        for side in range(HALVES):
            kv_arrive(sp - 2, side)
            if side == last:
                w_wait(1, dev_x, top)
                w_forward(8, dev_x, top, mate)
                w_wait(3, dev_y, bottom)
                w_forward(10, dev_y, bottom, mate)
            for turn in range(1, pairs):
                attend(turn, side)
    else:
        w_wait(1, dev_x, top)
        w_forward(8, dev_x, top, mate)
        w_wait(3, dev_y, bottom)
        w_forward(10, dev_y, bottom, mate)

    columns_each = w_ref.shape[1]

    def project(shard, squares):
        columns = pl.ds(pl.multiple_of(shard * columns_each, columns_each), columns_each)
        result = dot(att[...], w_all[shard])
        proj[:, columns] = result
        return squares + jnp.sum(result * result, axis=1, keepdims=True)

    mate_x, mate_y, mate_d = mate + flip_x, mate + flip_y, mate + flip_x + flip_y
    locals_[4].wait()
    w_wait(4, dev_d, top)
    w_forward(11, dev_d, top, mate)
    w_wait(5, dev_d, bottom)
    w_forward(12, dev_d, bottom, mate)
    squares = project(here, jnp.zeros((tokens, 1), F32))
    w_wait(6, mate, whole)
    squares = project(mate, squares)
    squares = project(dev_x, squares)
    squares = project(dev_y, squares)
    w_wait(7, mate_x, bottom)
    w_wait(8, mate_x, top)
    squares = project(mate_x, squares)
    w_wait(9, mate_y, top)
    w_wait(10, mate_y, bottom)
    squares = project(mate_y, squares)
    squares = project(dev_d, squares)
    w_wait(11, mate_d, top)
    w_wait(12, mate_d, bottom)
    squares = project(mate_d, squares)

    inverse = lax.rsqrt(squares * (1.0 / (columns_each * dp)) + EPSILON)
    for j in range(dp):
        columns = slice(j * columns_each, (j + 1) * columns_each)
        out_ref[:, columns] = (proj[:, columns] * inverse * og_ref[:, columns]).astype(BF16)

    for copy in sent:
        copy.wait_send()
    for step in range(sp - 1):
        for way in (0, 1):
            @pl.when(kv_sends(way, step))
            def _(way=way, step=step):
                for side in range(HALVES):
                    for copy in kv_copies(way, step, side):
                        copy.wait_send()


def per_device_fused(sp, dp, queries, keys, values, query_gain, key_gain, out_weight, out_gain):
    tokens = queries.shape[1]
    depth, columns = out_weight.shape
    hidden = queries.shape[2]
    kv_width = keys.shape[2]
    seq_len = tokens * sp
    hbm_spec = pl.BlockSpec(memory_space=pltpu.HBM)
    vmem_spec = pl.BlockSpec(memory_space=pltpu.VMEM)
    result = pl.pallas_call(
        functools.partial(kernel, sp, dp),
        out_shape=pltpu.VMEM((tokens, columns * dp), BF16),
        in_specs=[hbm_spec] * 3 + [vmem_spec] * 2 + [hbm_spec, vmem_spec, hbm_spec],
        out_specs=vmem_spec,
        scratch_shapes=[
            pltpu.VMEM((tokens, hidden), BF16),
            pltpu.VMEM((tokens, hidden), BF16),
            pltpu.VMEM((seq_len, kv_width), BF16),
            pltpu.VMEM((seq_len, kv_width), BF16),
            pltpu.VMEM((2, seq_len, 2 * HEAD), F32),
            pltpu.VMEM((dp, depth, columns), BF16),
            pltpu.VMEM((4, 16, BLOCK), F32),
            pltpu.VMEM((BLOCK, BLOCK), BF16),
            pltpu.VMEM((BLOCK, BLOCK), BF16),
            pltpu.VMEM((BLOCK, GROUP * tokens), BF16),
            pltpu.VMEM((tokens, GROUP * tokens), BF16),
            pltpu.VMEM((sp // 2, kv_width, 2 * tokens), BF16),
            pltpu.VMEM((max(sp // 2 - 1, 1), KVH, 2 * tokens, GROUP * tokens), F32),
            pltpu.VMEM((max(sp // 2 - 1, 1), KVH, 1, GROUP * tokens), F32),
            pltpu.VMEM((max(sp // 2 - 1, 1), KVH, 1, GROUP * tokens), F32),
            pltpu.VMEM((tokens, hidden), BF16),
            pltpu.VMEM((tokens, columns * dp), F32),
            pltpu.SemaphoreType.DMA((5,)),
            pltpu.SemaphoreType.DMA((2, sp - 1, HALVES, 2)),
            pltpu.SemaphoreType.DMA((2, sp - 1, HALVES, 2)),
            pltpu.SemaphoreType.DMA((13,)),
            pltpu.SemaphoreType.DMA((13,)),
        ],
        compiler_params=pltpu.CompilerParams(
            collective_id=0, has_side_effects=True, vmem_limit_bytes=66000000
        ),
    )(
        queries[0], keys[0], values[0], query_gain[None], key_gain[None],
        out_weight, out_gain[None], jnp.asarray(position_tables(seq_len)),
    )
    return result[None]


def solution(mesh):
    sp, dp = mesh.shape["sp"], mesh.shape["dp"]
    if dp == 8 and sp >= 2 and sp % 2 == 0 and sp <= 4:
        body = functools.partial(per_device_fused, sp, dp)
    else:
        body = per_device_general
    return jax.shard_map(
        body,
        mesh=mesh,
        in_specs=(
            P("dp", "sp", None),
            P("dp", "sp", None),
            P("dp", "sp", None),
            P(),
            P(),
            P(None, "dp"),
            P(),
        ),
        out_specs=P("dp", "sp", None),
        check_vma=False,
    )
```

profile of v0, /device:TPU:0, one launch (start us, length us, event | category | flops | bytes accessed | tf_op | source)
XLA Modules:
  0.0 27.1 jit_solution(657076598861610946)
XLA Ops:
  0.0 26.3 %shard_map.82 = bf16[192,2048]{1,0:T(8,128)(2,1)S(1)} custom-call(bf16[192,1024]{1,0:T(8,128)(2,1)} %bitcast.8, bf16[192,256]{1,0:T(8,128)(2,1)} %bitcast.9, bf16[192,256]{1,0:T(8,128)(2,1)} %bitcast.10, f32[1,64]{1,0:T(1,128)} %bitcast.12, f32[1,64]{1,0:T(1,128)} %bitcast.13, bf16[1024,256]{1,0:T(8,128)(2,1)} %w_ref.1, f32[1,2048]{1,0:T(1,128)} %bitcast.11, ...), custom_call_target="tpu_custom_call" | custom-call | tf_op jit(solution)/shard_map/pallas_call | solution.py:472
  26.3 0.9 %copy.10 = bf16[1,192,2048]{2,1,0:T(8,128)(2,1)} copy(bf16[1,192,2048]{2,1,0:T(8,128)(2,1)S(1)} %bitcast.7) | data formatting | bytes 1572864
where the time goes:
time: 27.3 us; the launch traced here: 27.1 us
  Pallas kernels  26.3 us (96%)
  local copies, waits for them, and re-layouts  0.88 us (3%)
    pallas_call x1, Pallas kernels, per_device_fused(): pl.pallas_call(functools.partial(kernel, sp, dp), out_shape=pltpu.VMEM((t...  26.3 us
    unnamed x1, local copies, waits for them, and re-layouts  0.88 us

commit v1 on v0

v1 whole, which is shorter than its diff:
```python
import functools

import jax
import jax.numpy as jnp
import numpy as np
from jax import lax
from jax.experimental import pallas as pl
from jax.experimental.pallas import tpu as pltpu
from jax.sharding import PartitionSpec as P

QH = 16
KVH = 4
HEAD = 64
GRID_W = 64
GROUP = QH // KVH
HALVES = 2
BLOCK = GROUP * HEAD
WIDTH = 128

TO_END = 64
TO_INNER = 160
CHUNKS = (256, 128, 128)
PIECES = 2 * (4 * len(CHUNKS) + 6) + 5


EPSILON = 1e-06
ROTARY_BASE = 10000.0

F32 = jnp.float32
BF16 = jnp.bfloat16


def rotate(vectors, positions, width):
    half_width = width // 2
    frequency = ROTARY_BASE ** (-jnp.arange(0, width, 2, dtype=jnp.float32) / width)
    angles = positions.astype(jnp.float32)[:, None] * frequency[None, :]
    cosines = jnp.cos(angles)[:, None, :]
    sine_table = jnp.sin(angles)[:, None, :]
    first_half = vectors[..., :half_width]
    second_half = vectors[..., half_width:]
    return jnp.concatenate(
        [
            first_half * cosines - second_half * sine_table,
            second_half * cosines + first_half * sine_table,
        ],
        axis=-1,
    )


def prepare(vectors, gain_vector, grid_row, grid_col):
    vectors = vectors.astype(jnp.float32)
    vectors = (
        vectors
        * lax.rsqrt(jnp.mean(vectors * vectors, axis=-1, keepdims=True) + EPSILON)
        * gain_vector
    )
    half_width = HEAD // 2
    turned = jnp.concatenate(
        [
            rotate(vectors[..., :half_width], grid_row, half_width),
            rotate(vectors[..., half_width:], grid_col, half_width),
        ],
        axis=-1,
    )
    return turned.astype(jnp.bfloat16)


def softmax_rows(scores):
    row_max = jnp.max(scores, axis=-1, keepdims=True)
    exponent = jnp.exp(scores - row_max)
    return exponent / jnp.sum(exponent, axis=-1, keepdims=True)


def per_device_general(queries, keys, values, query_gain, key_gain, out_weight, out_gain):
    sp_count = lax.axis_size("sp")
    tokens_here = queries.shape[1]
    seq_len = tokens_here * sp_count
    score_scale = HEAD ** (-0.5)
    offset = lax.axis_index("sp") * tokens_here
    positions = offset + jnp.arange(tokens_here, dtype=jnp.int32)
    grid_row = positions // GRID_W
    grid_col = positions % GRID_W
    query_rot = prepare(queries[0].reshape(tokens_here, QH, HEAD), query_gain, grid_row, grid_col)
    key_rot = prepare(keys[0].reshape(tokens_here, KVH, HEAD), key_gain, grid_row, grid_col)
    value_heads = values[0].reshape(tokens_here, KVH, HEAD)
    kv_pairs = jnp.concatenate([key_rot, value_heads], axis=2)
    all_pairs = lax.all_gather(
        kv_pairs.reshape(tokens_here, KVH * 2 * HEAD), "sp", axis=0, tiled=True
    )
    all_pairs = all_pairs.reshape(seq_len, KVH, 2, HEAD)
    key_all = all_pairs[:, :, 0].transpose(1, 0, 2)
    value_all = all_pairs[:, :, 1].transpose(1, 0, 2)
    query_groups = query_rot.reshape(tokens_here, KVH, QH // KVH, HEAD).transpose(1, 0, 2, 3)

    def attend_group(operands):
        query_group, key_head, value_head = operands
        scores = (
            jnp.einsum("qgd,kd->gqk", query_group, key_head, preferred_element_type=jnp.float32)
            * score_scale
        )
        attn_weights = softmax_rows(scores).astype(jnp.bfloat16)
        return jnp.einsum(
            "gqk,kd->qgd", attn_weights, value_head, preferred_element_type=jnp.float32
        ).astype(jnp.bfloat16)

    results = lax.map(attend_group, (query_groups, key_all, value_all))
    attended = results.transpose(1, 0, 2, 3).reshape(tokens_here, QH * HEAD)
    projected = jnp.dot(
        attended,
        lax.all_gather(out_weight, "dp", axis=1, tiled=True),
        preferred_element_type=jnp.float32,
    )
    normed = (
        projected
        * lax.rsqrt(jnp.mean(projected * projected, axis=-1, keepdims=True) + EPSILON)
        * out_gain
    )
    return normed.astype(jnp.bfloat16)[None]


def position_tables(seq_len):
    width = HEAD // 2
    frequency = np.float32(ROTARY_BASE) ** (
        -np.arange(0, width, 2, dtype=np.float32) / np.float32(width)
    )
    position = np.arange(seq_len)
    parts = []
    for coordinate in (position // GRID_W, position % GRID_W):
        angles = coordinate.astype(np.float32)[:, None] * frequency[None, :]
        parts += [angles, angles]
    angles = np.concatenate(parts * 2, axis=1).astype(np.float64)
    return np.stack([np.cos(angles), np.sin(angles)]).astype(np.float32)


def dot(a, b):
    return jnp.dot(a, b, preferred_element_type=F32)


def cross(a, b):
    return lax.dot_general(a, b, (((1,), (1,)), ((), ())), preferred_element_type=F32)


def kernel(
    sp, dp,
    q_ref, k_ref, v_ref, qg_ref, kg_ref, w_ref, og_ref, table_ref,
    out_ref,
    q_raw, k_all, v_all, tables, w_all, gains,
    swap_mat, ones_mat, q_t, v_turned,
    expo, peak, total, mixed, att, proj,
    local_sem, kv_send, kv_recv, w_send, w_recv,
):
    tokens = q_raw.shape[0]
    depth = w_ref.shape[0]
    half = depth // 2
    me = lax.axis_index("sp")
    here = lax.axis_index("dp")
    mate = here + 1 - 2 * (here % 2)
    flip_x = 2 - 4 * ((here // 2) % 2)
    flip_y = 4 - 8 * ((here // 4) % 2)
    dev_x = here + flip_x
    dev_y = here + flip_y
    dev_d = here + flip_x + flip_y

    barrier = pltpu.get_barrier_semaphore()
    has_left = me > 0
    has_right = me < sp - 1

    for other in (mate, dev_x, dev_y):
        pl.semaphore_signal(barrier, inc=1, device_id={"dp": other})

    @pl.when(has_left)
    def _():
        pl.semaphore_signal(barrier, inc=1, device_id={"sp": me - 1})

    @pl.when(has_right)
    def _():
        pl.semaphore_signal(barrier, inc=1, device_id={"sp": me + 1})

    locals_ = [
        pltpu.make_async_copy(k_ref, k_all.at[pl.ds(me * tokens, tokens)], local_sem.at[0]),
        pltpu.make_async_copy(v_ref, v_all.at[pl.ds(me * tokens, tokens)], local_sem.at[1]),
        pltpu.make_async_copy(w_ref, w_all.at[here], local_sem.at[2]),
        pltpu.make_async_copy(q_ref, q_raw, local_sem.at[3]),
        pltpu.make_async_copy(table_ref, tables, local_sem.at[4]),
    ]
    for copy in locals_:
        copy.start()
    for copy in locals_[:3]:
        copy.wait()

    pl.semaphore_wait(barrier, 3 + jnp.minimum(me, 1) + jnp.minimum(sp - 1 - me, 1))

    part = k_ref.shape[1] // HALVES

    stores = (k_all, v_all)

    def kv_copy(way, step, kind, side):
        block = me - step if way == 0 else me + step
        target = me + 1 if way == 0 else me - 1
        window = stores[kind].at[pl.ds(block * tokens, tokens), pl.ds(side * part, part)]
        return pltpu.make_async_remote_copy(
            src_ref=window,
            dst_ref=window,
            send_sem=kv_send.at[way, step, side, kind],
            recv_sem=kv_recv.at[way, step, side, kind],
            device_id={"sp": target},
        )

    def kv_sends(way, step):
        if way == 0:
            return jnp.logical_and(has_right, me - step >= 0)
        return jnp.logical_and(has_left, me + step < sp)

    def kv_start(way, step, kind, side):
        @pl.when(kv_sends(way, step))
        def _():
            kv_copy(way, step, kind, side).start()

    def kv_arrive(step, kind, side):
        for way in (0, 1):
            source = me - 1 - step if way == 0 else me + 1 + step
            arrives = source >= 0 if way == 0 else source < sp

            @pl.when(arrives)
            def _(way=way, source=source):
                window = stores[kind].at[
                    pl.ds(source * tokens, tokens), pl.ds(side * part, part)
                ]
                pltpu.make_async_remote_copy(
                    src_ref=window,
                    dst_ref=window,
                    send_sem=kv_send.at[way, step, side, kind],
                    recv_sem=kv_recv.at[way, step, side, kind],
                    device_id={"sp": me},
                ).wait_recv()

            if step + 1 < sp - 1:
                kv_start(way, step + 1, kind, side)

    for kind in (0, 1):
        for side in range(HALVES):
            for way in (1, 0):
                kv_start(way, 0, kind, side)

    odd = me % 2
    zmate = me + 1 - 2 * odd
    inner = (me + 1) // 2 % 2 == 1
    outer = jnp.logical_not(inner)
    shares = ((inner, 0, TO_END), (outer, half - TO_INNER, TO_INNER))
    mate_x, mate_y, mate_d = mate + flip_x, mate + flip_y, mate + flip_x + flip_y

    starts = [sum(CHUNKS[:j]) for j in range(len(CHUNKS))]
    pieces = {"own": (mate, 0, depth)}
    for j, (start, size) in enumerate(zip(starts, CHUNKS)):
        pieces["x", j] = (dev_x, half + start, size)
        pieces["y", j] = (dev_y, start, size)
        pieces["dx", j] = (dev_d, start, size)
        pieces["dy", j] = (dev_d, half + start, size)
    for name, shard, base in (("x", dev_x, 0), ("y", dev_y, half)):
        pieces[name, "middle"] = (shard, base + TO_END, half - TO_END - TO_INNER)
        for role, (_, start, size) in enumerate(shares):
            pieces[name, "share", role] = (shard, base + start, size)
    across = {"x": mate_x, "y": mate_y, "dx": mate_d, "dy": mate_d}
    for name in [name for name in pieces if name != "own"]:
        start, size = pieces[name][1:]
        pieces["mate", name] = (across[name[0]], start, size)
        if name[1] == "share":
            pieces["zed", name] = pieces[name]
    order = {name: i for i, name in enumerate(pieces)}
    sent = []

    def w_copy(name, shard, start, size, target):
        window = w_all.at[shard, pl.ds(start, size)]
        return pltpu.make_async_remote_copy(
            src_ref=window,
            dst_ref=window,
            send_sem=w_send.at[order[name]],
            recv_sem=w_recv.at[order[name]],
            device_id=target,
        )

    def w_give(name, shard, start, size, target):
        copy = w_copy(name, shard, start, size, target)
        copy.start()
        sent.append(copy)

    def w_own(name, target):
        w_give(name, here, *pieces[name][1:], {"dp": target})

    def w_wait(name):
        w_copy(name, *pieces[name], {"dp": mate}).wait_recv()

    def w_take(name):
        w_wait(name)
        piece = pieces[name]
        if name[1] in range(len(CHUNKS)):
            if name[0] == "x":
                w_give(("dy", name[1]), *piece, {"dp": dev_y})
            if name[0] == "y":
                w_give(("dx", name[1]), *piece, {"dp": dev_x})
        w_give(("mate", name), *piece, {"dp": mate})

    def w_share_own(name):
        for role, (chosen, _, _) in enumerate(shares):
            @pl.when(chosen)
            def _(key=(name, "share", role)):
                target = dev_x if name == "x" else dev_y
                w_copy(key, here, *pieces[key][1:], {"dp": target}).start()

    def w_share_near(name):
        for role, (chosen, _, _) in enumerate(shares):
            @pl.when(chosen)
            def _(key=(name, "share", role)):
                w_wait(key)
                w_copy(("zed", key), *pieces[key], {"sp": zmate}).start()
                w_copy(("mate", key), *pieces[key], {"dp": mate}).start()

    def w_share_far(name):
        for role in range(len(shares)):
            @pl.when(shares[1 - role][0])
            def _(key=(name, "share", role)):
                w_wait(("zed", key))
                w_copy(("mate", key), *pieces[key], {"dp": mate}).start()

    def w_share_sent(name):
        for role, (chosen, _, _) in enumerate(shares):
            key = (name, "share", role)
            w_copy(("mate", key), *pieces[key], {"dp": mate}).wait_send()

            @pl.when(chosen)
            def _(key=key):
                for form in (key, ("zed", key)):
                    w_copy(form, *pieces[key], {"dp": mate}).wait_send()

    for j in range(len(CHUNKS)):
        w_own(("x", j), dev_x)
        w_own(("y", j), dev_y)
    w_share_own("x")
    w_share_own("y")
    w_own(("x", "middle"), dev_x)
    w_own(("y", "middle"), dev_y)
    w_own("own", mate)

    row_id = lax.broadcasted_iota(jnp.int32, (BLOCK, BLOCK), 0)
    col_id = lax.broadcasted_iota(jnp.int32, (BLOCK, BLOCK), 1)
    quarter = HEAD // 4
    second = (col_id & (HEAD // 2 - 1)) >= quarter
    partner_col = jnp.where(second, col_id - quarter, col_id + quarter)
    hit = row_id == partner_col
    swap_mat[...] = jnp.where(hit, jnp.where(second, 1.0, -1.0), 0.0).astype(BF16)
    ones_mat[...] = jnp.where((row_id // HEAD) == (col_id // HEAD), 1.0, 0.0).astype(BF16)
    spread = jnp.where(
        row_id[:HEAD] == (col_id[:HEAD] & (HEAD - 1)), 1.0, 0.0
    ).astype(BF16)
    spread_swapped = jnp.where(
        row_id[:HEAD] == (partner_col[:HEAD] & (HEAD - 1)), 1.0, 0.0
    ).astype(BF16)
    for i, gain_ref in enumerate((qg_ref, kg_ref)):
        gain = jnp.broadcast_to(gain_ref[...], (16, HEAD))
        first = gain.astype(BF16)
        rest = gain - first.astype(F32)
        mid = rest.astype(BF16)
        low = (rest - mid.astype(F32)).astype(BF16)
        for j, matrix in enumerate((spread, spread_swapped)):
            gains[2 * i + j] = (dot(first, matrix) + dot(mid, matrix)) + dot(low, matrix)

    lane_head = lax.broadcasted_iota(jnp.int32, (1, BLOCK), 1) // HEAD
    masks = [jnp.where(lane_head == p, 1.0, 0.0).astype(BF16) for p in range(GROUP)]

    def turned(x, rows, which, scale):
        xf = x.astype(F32)
        square = xf * xf
        high = square.astype(BF16)
        low = (square - high.astype(F32)).astype(BF16)
        size = x.shape[1]
        ones = ones_mat[:size, :size]
        mean = (dot(high, ones) + dot(low, ones)) * (1.0 / HEAD)
        inverse = lax.rsqrt(mean + EPSILON) * scale
        swapped = dot(x, swap_mat[:size, :size])
        cosines = tables[0, rows, :]
        sines = tables[1, rows, :]
        if size > 2 * HEAD:
            cosines = jnp.concatenate([cosines, cosines], axis=1)
            sines = jnp.concatenate([sines, sines], axis=1)
        cosines = cosines * gains[2 * which, 0:1, :size]
        sines = sines * gains[2 * which + 1, 0:1, :size]
        return ((xf * cosines + swapped * sines) * inverse).astype(BF16)

    locals_[3].wait()
    locals_[4].wait()
    own_rows = pl.ds(pl.multiple_of(me * tokens, 64), tokens)
    for b in range(KVH):
        columns = slice(b * BLOCK, (b + 1) * BLOCK)
        query = turned(q_raw[:, columns], own_rows, 0, HEAD ** (-0.5))
        parts = [query[:WIDTH] * mask for mask in masks] + [query[WIDTH:] * mask for mask in masks]
        held = b % 2 * HEAD
        fold = jnp.where(row_id[:part] - held == (col_id[:part] & (HEAD - 1)), 1.0, 0.0)
        q_t[b] = cross(fold.astype(BF16), jnp.concatenate(parts, axis=0)).astype(BF16)

    eye = jnp.where(row_id == col_id, 1.0, 0.0).astype(BF16)
    far = 1 - me // 2
    blocks = [me, zmate, far + 1, 3 * far][:sp]
    spans = [pl.ds(pl.multiple_of(block * tokens, 64), tokens) for block in blocks]
    heads = KVH // HALVES
    rest = tokens - WIDTH
    final = sp - 1

    def score(turn, side):
        lanes = slice(side * part, (side + 1) * part)
        rows = spans[turn]
        key_side = turned(k_all[rows, lanes], rows, 1, 1.0)
        for b in range(side * heads, (side + 1) * heads):
            scores = dot(key_side, q_t[b])
            high = jnp.max(scores, axis=0, keepdims=True)
            if turn < final:
                weights = jnp.exp(scores - high)
                expo[turn, b] = weights
                peak[turn, b] = high
                total[turn, b] = jnp.sum(weights, axis=0, keepdims=True)
                continue
            for t in range(turn):
                high = jnp.maximum(high, peak[t, b])
            weights = jnp.exp(scores - high)
            norm = jnp.sum(weights, axis=0, keepdims=True)
            keeps = [jnp.exp(peak[t, b] - high) for t in range(turn)]
            for t in range(turn):
                norm = norm + total[t, b] * keeps[t]
            inverse = 1.0 / norm
            for t in range(turn):
                mixed[b, t * tokens : (t + 1) * tokens, :] = (
                    expo[t, b] * (keeps[t] * inverse)
                ).astype(BF16)
            mixed[b, turn * tokens :, :] = (weights * inverse).astype(BF16)

    def values(turn, side):
        lanes = slice(side * part, (side + 1) * part)
        pair = jnp.concatenate([v_all[spans[t], lanes] for t in (turn - 1, turn)], axis=0)
        width = slice((turn - 1) * tokens, (turn + 1) * tokens)
        v_turned[lanes, width] = cross(eye[:part, :part], pair).astype(BF16)

    def gather(side):
        for b in range(side * heads, (side + 1) * heads):
            value_rows = slice(b * HEAD, (b + 1) * HEAD)
            product = dot(v_turned[value_rows, :], mixed[b])
            for p in range(0, GROUP, 2):
                lanes = slice(b * BLOCK + p * HEAD, b * BLOCK + (p + 2) * HEAD)
                two = [product[:, i * WIDTH : (i + 1) * WIDTH] for i in (p, p + 1)]
                att[:WIDTH, lanes] = jnp.concatenate(two, axis=0).T.astype(BF16)
                start = GROUP * WIDTH + p * rest
                two = product[:, start : start + 2 * rest].T
                two = jnp.concatenate([two[:rest], two[rest:]], axis=1)
                att[WIDTH:, lanes] = two.astype(BF16)

    lots = len(CHUNKS)
    columns_each = w_ref.shape[1]
    late = CHUNKS[-1]
    tails = [half - late, depth - late]

    def columns_of(shard):
        return pl.ds(pl.multiple_of(shard * columns_each, columns_each), columns_each)

    def product(shard, start, size):
        rows = pl.ds(start, size)
        return dot(att[:, rows], w_all[shard, rows, :])

    def finish(shard, result, squares):
        proj[:, columns_of(shard)] = result
        return squares + jnp.sum(result * result, axis=1, keepdims=True)

    def project(shard, squares):
        return finish(shard, dot(att[...], w_all[shard]), squares)

    def begin(shard):
        proj[:, columns_of(shard)] = product(shard, 0, half - late) + product(
            shard, half, half - late
        )

    def end(shard, squares):
        result = proj[:, columns_of(shard)]
        for start in tails:
            result = result + product(shard, start, late)
        return finish(shard, result, squares)

    def take(*names):
        for name in names:
            w_take(("x", name))
            w_take(("y", name))

    def take_far(j):
        w_take(("dx", j))
        w_take(("dy", j))

    for side in range(HALVES):
        score(0, side)
    for step in range(sp - 1):
        last = step == sp - 2
        for side in range(HALVES):
            kv_arrive(step, 0, side)
            score(step + 1, side)
            if step == 0 and side == 0:
                take(0)
        for side in range(HALVES):
            kv_arrive(step, 1, side)
            if (step + 1) % 2:
                values(step + 1, side)
            if last:
                gather(side)
                if side == 0:
                    take_far(0)
            elif step == 0:
                take(side + 1)
        if step == max(sp - 3, 0):
            w_share_near("x")
            w_share_near("y")
            take("middle")

    squares = project(here, jnp.zeros((tokens, 1), F32))
    w_wait("own")
    squares = project(mate, squares)
    for j in range(1, lots - 1):
        take_far(j)
    for name in ("x", "y"):
        w_share_far(name)
    squares = project(dev_x, squares)
    squares = project(dev_y, squares)
    take_far(lots - 1)
    squares = project(dev_d, squares)
    for name, shard in (("x", mate_x), ("y", mate_y)):
        for piece in (*range(lots), "middle"):
            w_wait(("mate", (name, piece)))
        for role in range(len(shares)):
            w_wait(("mate", (name, "share", role)))
        squares = project(shard, squares)
    for j in range(lots - 1):
        w_wait(("mate", ("dx", j)))
        w_wait(("mate", ("dy", j)))
    begin(mate_d)
    w_wait(("mate", ("dx", lots - 1)))
    w_wait(("mate", ("dy", lots - 1)))
    squares = end(mate_d, squares)

    inverse = lax.rsqrt(squares * (1.0 / (columns_each * dp)) + EPSILON)
    for j in range(dp):
        columns = slice(j * columns_each, (j + 1) * columns_each)
        out_ref[:, columns] = (proj[:, columns] * inverse * og_ref[:, columns]).astype(BF16)

    for copy in sent:
        copy.wait_send()
    for name in ("x", "y"):
        w_share_sent(name)
    for step in range(sp - 1):
        for way in (0, 1):
            @pl.when(kv_sends(way, step))
            def _(way=way, step=step):
                for kind in (0, 1):
                    for side in range(HALVES):
                        kv_copy(way, step, kind, side).wait_send()


def per_device_fused(sp, dp, queries, keys, values, query_gain, key_gain, out_weight, out_gain):
    tokens = queries.shape[1]
    depth, columns = out_weight.shape
    hidden = queries.shape[2]
    kv_width = keys.shape[2]
    seq_len = tokens * sp
    hbm_spec = pl.BlockSpec(memory_space=pltpu.HBM)
    vmem_spec = pl.BlockSpec(memory_space=pltpu.VMEM)
    result = pl.pallas_call(
        functools.partial(kernel, sp, dp),
        out_shape=pltpu.VMEM((tokens, columns * dp), BF16),
        in_specs=[hbm_spec] * 3 + [vmem_spec] * 2 + [hbm_spec, vmem_spec, hbm_spec],
        out_specs=vmem_spec,
        scratch_shapes=[
            pltpu.VMEM((tokens, hidden), BF16),
            pltpu.VMEM((seq_len, kv_width), BF16),
            pltpu.VMEM((seq_len, kv_width), BF16),
            pltpu.VMEM((2, seq_len, 2 * HEAD), F32),
            pltpu.VMEM((dp, depth, columns), BF16),
            pltpu.VMEM((4, 16, BLOCK), F32),
            pltpu.VMEM((BLOCK, BLOCK), BF16),
            pltpu.VMEM((BLOCK, BLOCK), BF16),
            pltpu.VMEM((KVH, kv_width // HALVES, GROUP * tokens), BF16),
            pltpu.VMEM((kv_width, seq_len), BF16),
            pltpu.VMEM((sp - 1, KVH, tokens, GROUP * tokens), F32),
            pltpu.VMEM((sp - 1, KVH, 1, GROUP * tokens), F32),
            pltpu.VMEM((sp - 1, KVH, 1, GROUP * tokens), F32),
            pltpu.VMEM((KVH, seq_len, GROUP * tokens), BF16),
            pltpu.VMEM((tokens, hidden), BF16),
            pltpu.VMEM((tokens, columns * dp), F32),
            pltpu.SemaphoreType.DMA((5,)),
            pltpu.SemaphoreType.DMA((2, sp - 1, HALVES, 2)),
            pltpu.SemaphoreType.DMA((2, sp - 1, HALVES, 2)),
            pltpu.SemaphoreType.DMA((PIECES,)),
            pltpu.SemaphoreType.DMA((PIECES,)),
        ],
        compiler_params=pltpu.CompilerParams(
            collective_id=0, has_side_effects=True, vmem_limit_bytes=66000000
        ),
    )(
        queries[0], keys[0], values[0], query_gain[None], key_gain[None],
        out_weight, out_gain[None], jnp.asarray(position_tables(seq_len)),
    )
    return result[None]


def solution(mesh):
    sp, dp = mesh.shape["sp"], mesh.shape["dp"]
    if dp == 8 and sp >= 2 and sp % 2 == 0 and sp <= 4:
        body = functools.partial(per_device_fused, sp, dp)
    else:
        body = per_device_general
    return jax.shard_map(
        body,
        mesh=mesh,
        in_specs=(
            P("dp", "sp", None),
            P("dp", "sp", None),
            P("dp", "sp", None),
            P(),
            P(),
            P(None, "dp"),
            P(),
        ),
        out_specs=P("dp", "sp", None),
        check_vma=False,
    )
```

time: 27.3 us -> 26.7 us (0.978)
  the two profiles are of different devices: /device:TPU:0 before, /device:TPU:1 now
where the time goes in v1:
time: 26.7 us; the launch traced here: 26.5 us
  Pallas kernels  25.6 us (96%)
  local copies, waits for them, and re-layouts  0.88 us (3%)
    pallas_call x1, Pallas kernels, per_device_fused(): pl.pallas_call(functools.partial(kernel, sp, dp), out_shape=pltpu.VMEM((t...  25.6 us
    unnamed x1, local copies, waits for them, and re-layouts  0.88 us

profile of v1, /device:TPU:1, one launch (start us, length us, event | category | flops | bytes accessed | tf_op | source)
XLA Modules:
  0.0 26.5 jit_solution(4539260073132139128)
XLA Ops:
  0.0 25.6 %shard_map.82 = bf16[192,2048]{1,0:T(8,128)(2,1)S(1)} custom-call(bf16[192,1024]{1,0:T(8,128)(2,1)} %bitcast.8, bf16[192,256]{1,0:T(8,128)(2,1)} %bitcast.9, bf16[192,256]{1,0:T(8,128)(2,1)} %bitcast.10, f32[1,64]{1,0:T(1,128)} %bitcast.12, f32[1,64]{1,0:T(1,128)} %bitcast.13, bf16[1024,256]{1,0:T(8,128)(2,1)} %w_ref.1, f32[1,2048]{1,0:T(1,128)} %bitcast.11, ...), custom_call_target="tpu_custom_call" | custom-call | tf_op jit(solution)/shard_map/pallas_call | solution.py:568
  25.6 0.9 %copy.10 = bf16[1,192,2048]{2,1,0:T(8,128)(2,1)} copy(bf16[1,192,2048]{2,1,0:T(8,128)(2,1)S(1)} %bitcast.7) | data formatting | bytes 1572864
